TPU v7x, 128 devices: a whole 4x4x4 slice. The times are simulated.
128 devices in a mesh: sp: 32 (over z, y, core), tp: 4 (over x).
Axes of the slice: x: 4, y: 4, z: 4, core: 2. Of those that a mesh axis runs over, the one named last changes fastest.
Arguments:
- residual: bfloat16 [12288, 2048], P('sp'), may hold values from -50 to 50
- queries_a: bfloat16 [12288, 512], P('sp', 'tp'), may hold values from -50 to 50
- keys_a: bfloat16 [12288, 512], P('sp', 'tp'), may hold values from -9 to 9
- values_a: bfloat16 [12288, 512], P('sp', 'tp'), may hold values from -6 to 6
- queries_b: bfloat16 [12288, 1024], P('sp', 'tp'), may hold values from -50 to 50
- keys_b: bfloat16 [12288, 1024], P('sp', 'tp'), may hold values from -9 to 9
- values_b: bfloat16 [12288, 512], P('sp', 'tp'), may hold values from -6 to 6
- mix_lambda: float32 [2, 4], P(None, 'tp'), may hold values from 0.3 to 0.8
- head_gain: float32 [2, 128], replicated, may hold values from 0.1 to 1.9
- out_a: bfloat16 [512, 2048], P('tp'), may hold values from -0.1875 to 0.1875
- out_b: bfloat16 [512, 2048], P('tp'), may hold values from -0.1875 to 0.1875
- norm_gain: float32 [2048], replicated, may hold values from 0.1 to 1.9
- w_gate: bfloat16 [2048, 5632], P('sp', 'tp'), may hold values from -0.125 to 0.125
- w_up: bfloat16 [2048, 5632], P('sp', 'tp'), may hold values from -0.125 to 0.125
- w_down: bfloat16 [5632, 2048], P('tp', 'sp'), may hold values from -0.21875 to 0.21875
Outputs:
- layer_out: bfloat16 [12288, 2048], P('sp', 'tp')
All inputs are finite; a program needn't handle non-finite values.
Results may differ from a plain program's by a relative error of at most 0.0085.
Values may be sent and summed in bfloat16 or wider, within the bound.
A program may use at most 256 MiB of HBM per device.

v0:
```python
import functools

import jax
import jax.numpy as jnp
from jax import lax
from jax.experimental import pallas as pl
from jax.experimental.pallas import tpu as pltpu
from jax.sharding import PartitionSpec as P

MESH = pl.DeviceIdType.MESH
F32 = jnp.float32
BF16 = jnp.bfloat16
eps_norm = 1e-06
head_scale = 0.8
log2e = 1.4426950408889634
OFFS = (0, -1, 1, 2)


class Place:
    def __init__(self):
        self.x = lax.axis_index("tp")
        self.me = lax.axis_index("sp")
        self.c = self.me % 2
        y = (self.me // 2) % 4
        z = self.me // 8
        self.z = z
        self.p = y * (1 - self.c) + z * self.c
        self.s = z * (1 - self.c) + y * self.c

    def own(self, dp, ds):
        p, s, c = (self.p + dp + 4) % 4, (self.s + ds + 4) % 4, self.c
        return ((1 - c) * (4 * s + p) + c * (4 * p + s)) * 2 + c

    def other(self, dp, ds):
        p, s, c = (self.s + dp + 4) % 4, (self.p + ds + 4) % 4, 1 - self.c
        return ((1 - c) * (4 * s + p) + c * (4 * p + s)) * 2 + c

    def ring(self, dx):
        return (self.me, (self.x + dx + 4) % 4)


def remote(view, send, recv, device):
    return pltpu.make_async_remote_copy(
        src_ref=view,
        dst_ref=view,
        send_sem=send,
        recv_sem=recv,
        device_id=device,
        device_id_type=MESH,
    )


class Plane:
    count = 36

    def __init__(self, place, whole, half, send, recv):
        self.at, self.whole, self.half, self.send, self.recv = place, whole, half, send, recv

    def copy(self, n):
        at = self.at
        if n < 2:
            view, to = self.whole(at.own(0, 0)), at.own(1 - 2 * n, 0)
        elif n < 4:
            view = self.half(at.own(-1 if n == 2 else 1, 0), n - 2)
            to = at.own(1 if n == 2 else -1, 0)
        elif n < 12:
            view = self.whole(at.own(OFFS[n % 4], 0))
            to = at.own(0, 1 if n < 8 else -1)
        elif n < 20:
            low = n < 16
            view = self.half(at.own(OFFS[n % 4], -1 if low else 1), 0 if low else 1)
            to = at.own(0, 1 if low else -1)
        else:
            view = self.whole(at.own(OFFS[n % 4], (0, -1, 1, 2)[(n - 20) // 4]))
            to = at.other(0, 0)
        return remote(view, self.send.at[n], self.recv.at[n], (to, at.x))

    def go(self, *ns):
        for n in ns:
            self.copy(n).start()

    def come(self, *ns):
        for n in ns:
            self.copy(n).wait_recv()

    def start(self):
        self.go(0, 1, 4, 8, 20)

    def event(self, e):
        line, i = e // 4, e % 4
        if e == 1:
            self.come(0)
            self.go(2, 5, 9)
        elif e == 2:
            self.come(1)
            self.go(3, 6, 10)
        elif e == 3:
            self.come(2, 3)
            self.go(7, 11)
        elif line == 1:
            self.come(4 + i)
            self.go(12 + i)
        elif line == 2:
            self.come(8 + i)
            self.go(16 + i)
        else:
            self.come(12 + i, 16 + i)
        self.go(20 + e)

    def own_block(self, e):
        return self.at.own(OFFS[e % 4], (0, -1, 1, 2)[e // 4])

    def other_block(self, e):
        return self.at.other(OFFS[e % 4], (0, -1, 1, 2)[e // 4])

    def shared(self, e):
        self.come(20 + e)

    def drain(self):
        for n in range(self.count):
            self.copy(n).wait_send()


class Ring:
    def __init__(self, place, whole, half, send, recv, share):
        self.at, self.whole, self.half = place, whole, half
        self.send, self.recv, self.share = send, recv, share

    def copy(self, n):
        at = self.at
        if n < 2:
            view, to = self.whole(at.x), at.ring(1 - 2 * n)
        elif n < 4:
            view = self.half((at.x + (3 if n == 2 else 1)) % 4, n - 2)
            to = at.ring(1 if n == 2 else -1)
        else:
            view, to = self.whole((at.x + (3, 1, 2)[n - 4]) % 4), (at.other(0, 0), at.x)
        return remote(view, self.send.at[n], self.recv.at[n], to)

    def start(self):
        self.copy(0).start()
        self.copy(1).start()

    def relay(self):
        for n in (0, 1):
            self.copy(n).wait_recv()
            self.copy(n + 2).start()
            if self.share:
                self.copy(n + 4).start()

    def last(self):
        self.copy(2).wait_recv()
        self.copy(3).wait_recv()
        if self.share:
            self.copy(6).start()

    def shared(self):
        for n in (4, 5, 6):
            self.copy(n).wait_recv()

    def drain(self):
        for n in range(7 if self.share else 4):
            self.copy(n).wait_send()


RECV = (1, 2, 4, 8, 3, 5, 9, 6, 10, 12, 7, 11, 13, 14, 15)
LAG = 3


def steps():
    order = [("own", 0), ("other", 0)]
    for k in range(len(RECV) + LAG):
        if k < len(RECV):
            order.append(("own", RECV[k]))
        if k >= LAG:
            order.append(("other", RECV[k - LAG]))
    return order


CHUNKS = ((0, 0), (0, 384), (1, 0), (2, 384))


def attend(kv, q_a, q_b, peak, denom, numer, rows):
    key_a = kv[0:rows, 0:128]
    key_1 = kv[0:rows, 128:256]
    key_2 = kv[0:rows, 256:384]
    left = [jnp.concatenate([k, k], 1) for k in (key_a, key_1, key_2)]
    value = [kv[rows : rows + 128, :], kv[rows + 128 : rows + 256, :]]

    def score(chunk):
        which, at = chunk
        q = q_a if which == 0 else q_b
        return jnp.dot(left[which], q[:, at : at + rows], preferred_element_type=F32)

    coming = score(CHUNKS[0])
    for k, (which, at) in enumerate(CHUNKS):
        scores = coming
        if k + 1 < len(CHUNKS):
            coming = score(CHUNKS[k + 1])
        group = min(which, 1)
        cols = slice(at + 2 * rows * group, at + 2 * rows * group + rows)
        before = peak[0:1, cols]
        fresh = jnp.maximum(before, jnp.max(scores, axis=0, keepdims=True))
        decay = jnp.exp2(before - fresh)
        weights = jnp.exp2(scores - fresh)
        peak[0:1, cols] = fresh
        denom[0:1, cols] = denom[0:1, cols] * decay + jnp.sum(weights, axis=0, keepdims=True)
        added = jnp.dot(value[group], weights.astype(BF16), preferred_element_type=F32)
        numer[:, cols] = numer[:, cols] * decay + added


def hi_lo(q, scale):
    wide = jnp.transpose(q.astype(F32) * scale)
    high = wide.astype(BF16).astype(F32)
    return high, wide - high


def kernel(
    residual, queries_a, keys_a, values_a, queries_b, keys_b, values_b, lambdas, head_gain,
    out_a, out_b, norm_gain, w_gate, w_up, w_down, out,
    kv, gu, dn, ow, heads, part, came, res, q_in, v_in, d_in, q_a, q_b, peak, denom, numer,
    summed, normed, gates, hidden, square,
    kv_send, kv_recv, gu_send, gu_recv, dn_send, dn_recv, ow_send, ow_recv,
    hd_send, hd_recv, rs_send, rs_recv, load,
):
    at = Place()
    me, x = at.me, at.x
    rows = residual.shape[0]
    depth = w_gate.shape[0]
    share = out.shape[1]
    inner = w_gate.shape[1]

    def local(n, src, dst):
        return pltpu.make_async_copy(src, dst, load.at[n])

    loads = [
        local(0, keys_a, kv.at[me, 0:rows, 0:128]),
        local(1, keys_b, kv.at[me, 0:rows, 128:384]),
        local(2, values_a, v_in.at[0]),
        local(3, values_b, v_in.at[1]),
        local(4, queries_a, q_in.at[:, 0:128]),
        local(5, queries_b, q_in.at[:, 128:384]),
        local(6, out_a, ow.at[x, 0]),
        local(7, out_b, ow.at[x, 1]),
        local(8, w_gate, gu.at[0, me]),
        local(9, w_up, gu.at[1, me]),
        local(10, w_down, d_in),
        local(11, residual, res),
    ]
    for c in loads:
        c.start()

    barrier = pltpu.get_barrier_semaphore()
    friends = [(at.own(1, 0), x), (at.own(-1, 0), x), (at.own(0, 1), x), (at.own(0, -1), x)]
    friends += [(at.other(0, 0), x), at.ring(1), at.ring(2), at.ring(-1)]
    for f in friends:
        pl.semaphore_signal(barrier, inc=1, device_id=f, device_id_type=MESH)

    for n in (2, 3):
        loads[n].wait()
    for g in range(2):
        kv[me, rows + 128 * g : rows + 128 * (g + 1), :] = jnp.transpose(
            v_in[g].astype(F32)
        ).astype(BF16)
    for n in (0, 1):
        loads[n].wait()
    pl.semaphore_wait(barrier, len(friends))

    cut = (rows + 256) // 2
    KV = Plane(
        at, lambda b: kv.at[b], lambda b, h: kv.at[b, cut * h : cut * (h + 1)], kv_send, kv_recv
    )
    mid = depth // 2
    GU = Plane(
        at,
        lambda b: gu.at[:, b],
        lambda b, h: gu.at[:, b, mid * h : mid * (h + 1)],
        gu_send,
        gu_recv,
    )
    DN = Plane(
        at, lambda b: dn.at[b], lambda b, h: dn.at[b, mid * h : mid * (h + 1)], dn_send, dn_recv
    )
    OW = Ring(
        at,
        lambda b: ow.at[b, at.c],
        lambda b, h: ow.at[b, at.c, 64 * h : 64 * (h + 1)],
        ow_send,
        ow_recv,
        True,
    )
    HD = Ring(
        at,
        lambda b: heads.at[b],
        lambda b, h: heads.at[b, rows // 2 * h : rows // 2 * (h + 1)],
        hd_send,
        hd_recv,
        False,
    )
    KV.start()
    for n in (6, 7):
        loads[n].wait()
    OW.start()

    for n in (4, 5):
        loads[n].wait()
    high, low = hi_lo(q_in[:, 0:128], log2e / 8.0)
    first = lax.broadcasted_iota(jnp.int32, high.shape, 0) < 64
    for j in range(2):
        keep = first if j == 0 else jnp.logical_not(first)
        cols = slice(rows * j, rows * (j + 1))
        q_a[0:128, cols] = jnp.where(keep, high, 0.0).astype(BF16)
        q_a[128:256, cols] = jnp.where(keep, low, 0.0).astype(BF16)
        high_b, low_b = hi_lo(q_in[:, 128 * (j + 1) : 128 * (j + 2)], log2e * 128.0**-0.5)
        q_b[0:128, cols] = high_b.astype(BF16)
        q_b[128:256, cols] = low_b.astype(BF16)
    peak[...] = jnp.full(peak.shape, -1e30, F32)
    denom[...] = jnp.zeros(denom.shape, F32)
    numer[...] = jnp.zeros(numer.shape, F32)
    loads[10].wait()
    dn[me] = jnp.transpose(d_in[...].astype(F32)).astype(BF16)
    for n in (8, 9, 11):
        loads[n].wait()

    order = steps()

    def step(i, carry):
        block = 0
        for k, (whose, e) in enumerate(order):
            b = KV.own_block(e) if whose == "own" else KV.other_block(e)
            block = block + jnp.where(i == k, b, 0)
            if e == 0 and whose == "own":
                continue

            @pl.when(i == k)
            def _(whose=whose, e=e, k=k):
                if whose == "own":
                    KV.event(e)
                    if e == 11:
                        GU.start()
                else:
                    KV.shared(e)
                if k == 10:
                    OW.relay()
                if k == 20:
                    OW.last()

        attend(kv.at[block], q_a, q_b, peak, denom, numer, rows)
        return carry

    lax.fori_loop(0, len(order), step, 0)

    for e in (1, 2, 4, 8):
        GU.event(e)
    ratio = numer[...] / denom[0:1, :]
    for g in range(2):
        base = 2 * rows * g
        mixed = ratio[:, base : base + rows] - lambdas[g, 0] * ratio[:, base + rows : base + 2 * rows]
        scale = lax.rsqrt(jnp.mean(mixed * mixed, axis=0, keepdims=True) + eps_norm)
        done = jnp.transpose(mixed * scale) * head_gain[g : g + 1, :] * head_scale
        heads[x, :, 128 * g : 128 * (g + 1)] = done.astype(BF16)
    HD.start()
    for e in (3, 5, 9):
        GU.event(e)
    HD.relay()
    for e in (6, 10, 12):
        GU.event(e)
    HD.last()
    OW.shared()

    wide = summed.shape[1]
    square[...] = jnp.zeros(square.shape, F32)

    @pl.loop(0, wide // 256)
    def _(n):
        cols = pl.ds(pl.multiple_of(n * 256, 256), 256)
        left = jnp.concatenate([heads[k] for k in range(4)], axis=1)
        right = ow[:, :, :, cols].reshape(1024, 256)
        total = res[:, cols].astype(F32) + jnp.dot(left, right, preferred_element_type=F32)
        summed[:, cols] = total
        twice = total * total
        square[...] += twice[:, 0:128] + twice[:, 128:256]

    inverse = lax.rsqrt(jnp.sum(square[...], axis=1, keepdims=True) / wide + eps_norm)

    @pl.loop(0, wide // 256)
    def _(n):
        cols = pl.ds(pl.multiple_of(n * 256, 256), 256)
        normed[:, cols] = (summed[:, cols] * inverse * norm_gain[0:1, cols]).astype(BF16)

    for e in (7, 11, 13, 14, 15):
        GU.event(e)
        if e == 11:
            DN.start()
    for e in range(16):
        GU.shared(e)

    gates[...] = jnp.zeros(gates.shape, F32)
    pieces = ((0, 512), (512, 512), (1024, inner - 1024))

    @pl.loop(0, 4)
    def _(k):
        left = normed[:, pl.ds(pl.multiple_of(k * 512, 512), 512)]
        for g in range(2):
            for lo, n in pieces:
                right = gu[g, pl.ds(k * 8, 8), :, lo : lo + n].reshape(8 * depth, n)
                gates[g, :, lo : lo + n] += jnp.dot(left, right, preferred_element_type=F32)

    for e in (1, 2, 4, 8, 3, 5, 9, 6, 10, 12):
        DN.event(e)
    for lo, n in pieces:
        gate = gates[0, :, lo : lo + n]
        hidden[:, lo : lo + n] = (gate / (1.0 + jnp.exp(-gate)) * gates[1, :, lo : lo + n]).astype(BF16)
    for e in (7, 11, 13, 14, 15):
        DN.event(e)
    for e in range(16):
        DN.shared(e)

    def give(n):
        return pltpu.make_async_remote_copy(
            src_ref=part.at[(x + n + 1) % 4],
            dst_ref=came.at[n],
            send_sem=rs_send.at[n],
            recv_sem=rs_recv.at[n],
            device_id=at.ring(n + 1),
            device_id_type=MESH,
        )

    for n in (1, 0, 2, 3):
        to = (x + n + 1) % 4
        right = dn[pl.ds(to * 8, 8)].reshape(share, inner)
        sums = lax.dot_general(
            hidden[...], right, (((1,), (1,)), ((), ())), preferred_element_type=F32
        )
        part[to] = sums.astype(BF16)
        if n < 3:
            give(n).start()
    total = part[x].astype(F32)
    for n in range(3):
        give(n).wait_recv()
        total = total + came[n].astype(F32)
    mine = summed[:, pl.ds(pl.multiple_of(x * share, share), share)]
    out[...] = (mine + 0.5 * total).astype(BF16)

    for gather in (KV, GU, DN, OW, HD):
        gather.drain()
    for n in range(3):
        give(n).wait_send()


def local(
    residual, queries_a, keys_a, values_a, queries_b, keys_b, values_b, mix_lambda, head_gain,
    out_a, out_b, norm_gain, w_gate, w_up, w_down,
):
    rows, wide = residual.shape
    depth, inner = w_gate.shape
    share = wide // 4
    anywhere = pl.BlockSpec(memory_space=pl.ANY)
    vmem = pl.BlockSpec(memory_space=pltpu.VMEM)
    smem = pl.BlockSpec(memory_space=pltpu.SMEM)
    dma = pltpu.SemaphoreType.DMA
    count = Plane.count
    return pl.pallas_call(
        kernel,
        out_shape=jax.ShapeDtypeStruct((rows, share), BF16),
        in_specs=[anywhere] * 7 + [smem, vmem, anywhere, anywhere, vmem] + [anywhere] * 3,
        out_specs=vmem,
        scratch_shapes=[
            pltpu.VMEM((32, rows + 256, rows), BF16),
            pltpu.VMEM((2, 32, depth, inner), BF16),
            pltpu.VMEM((32, depth, inner), BF16),
            pltpu.VMEM((4, 2, 128, wide), BF16),
            pltpu.VMEM((4, rows, 256), BF16),
            pltpu.VMEM((4, rows, share), BF16),
            pltpu.VMEM((3, rows, share), BF16),
            pltpu.VMEM((rows, wide), BF16),
            pltpu.VMEM((rows, 384), BF16),
            pltpu.VMEM((2, rows, 128), BF16),
            pltpu.VMEM((inner, depth), BF16),
            pltpu.VMEM((256, 2 * rows), BF16),
            pltpu.VMEM((256, 2 * rows), BF16),
            pltpu.VMEM((1, 4 * rows), F32),
            pltpu.VMEM((1, 4 * rows), F32),
            pltpu.VMEM((128, 4 * rows), F32),
            pltpu.VMEM((rows, wide), F32),
            pltpu.VMEM((rows, wide), BF16),
            pltpu.VMEM((2, rows, inner), F32),
            pltpu.VMEM((rows, inner), BF16),
            pltpu.VMEM((rows, 128), F32),
            dma((count,)), dma((count,)), dma((count,)), dma((count,)), dma((count,)), dma((count,)),
            dma((7,)), dma((7,)), dma((4,)), dma((4,)), dma((3,)), dma((3,)),
            dma((12,)),
        ],
        compiler_params=pltpu.CompilerParams(
            collective_id=0, has_side_effects=True, vmem_limit_bytes=67043328
        ),
        name="layer",
    )(
        residual, queries_a, keys_a, values_a, queries_b, keys_b, values_b, mix_lambda, head_gain,
        out_a, out_b, norm_gain.reshape(1, wide), w_gate, w_up, w_down,
    )


def solution(mesh):
    in_specs = (
        P("sp", None),
        P("sp", "tp"),
        P("sp", "tp"),
        P("sp", "tp"),
        P("sp", "tp"),
        P("sp", "tp"),
        P("sp", "tp"),
        P(None, "tp"),
        P(),
        P("tp", None),
        P("tp", None),
        P(),
        P("sp", "tp"),
        P("sp", "tp"),
        P("tp", "sp"),
    )
    return jax.shard_map(
        local, mesh=mesh, in_specs=in_specs, out_specs=P("sp", "tp"), check_vma=False
    )
```

profile of v0, /device:TPU:5, one launch (start us, length us, event | category | flops | bytes accessed | tf_op | source)
XLA Modules:
  0.0 144.0 jit_solution(10398423534482696874)
XLA Ops:
  0.0 1.3 copy.16.lambdas
  1.3 1.8 %copy.17.w_down = bf16[1408,64]{1,0:T(8,128)(2,1)} copy(bf16[1408,64]{0,1:T(8,128)(2,1)} %param.29) | data formatting | bytes 360448 | tf_op args[14]
  3.1 139.1 %layer.1 = bf16[384,512]{1,0:T(8,128)(2,1)} custom-call(bf16[384,2048]{1,0:T(8,128)(2,1)} %residual.1, bf16[384,128]{1,0:T(8,128)(2,1)} %queries_a.1, bf16[384,128]{1,0:T(8,128)(2,1)} %keys_a.1, bf16[384,128]{1,0:T(8,128)(2,1)} %values_a.1, bf16[384,256]{1,0:T(8,128)(2,1)} %queries_b.1, bf16[384,256]{1,0:T(8,128)(2,1)} %keys_b.1, bf16[384,128]{1,0:T(8,128)(2,1)} %values_b.1, ...), custom_call_target="tpu_custom_call" | custom-call | tf_op jit(solution)/shard_map/layer/pallas_call | solution.py:463
  142.2 1.8 %copy.19 = bf16[384,512]{1,0:T(8,128)(2,1)} copy(bf16[384,512]{1,0:T(8,128)(2,1)} %layer.1) | data formatting | bytes 786432
where the time goes:
time: 146 us; the launch traced here: 144 us
  Pallas kernels  139 us (95%)
  local copies, waits for them, and re-layouts  4.91 us (3%)
    pallas_call x1, Pallas kernels, local(): pl.pallas_call(kernel, out_shape=jax.ShapeDtypeStruct((rows, share), BF16...  139 us
    unnamed x3, local copies, waits for them, and re-layouts  4.91 us

commit v1 on v0

v1 whole, which is shorter than its diff:
```python
import functools

import jax
import jax.numpy as jnp
from jax import lax
from jax.experimental import pallas as pl
from jax.experimental.pallas import tpu as pltpu
from jax.sharding import PartitionSpec as P

MESH = pl.DeviceIdType.MESH
F32 = jnp.float32
BF16 = jnp.bfloat16
eps_norm = 1e-06
head_scale = 0.8
log2e = 1.4426950408889634
OFFS = (0, -1, 1, 2)


class Place:
    def __init__(self):
        self.x = lax.axis_index("tp")
        self.me = lax.axis_index("sp")
        self.c = self.me % 2
        y = (self.me // 2) % 4
        z = self.me // 8
        self.z = z
        self.p = y * (1 - self.c) + z * self.c
        self.s = z * (1 - self.c) + y * self.c

    def own(self, dp, ds):
        p, s, c = (self.p + dp + 4) % 4, (self.s + ds + 4) % 4, self.c
        return ((1 - c) * (4 * s + p) + c * (4 * p + s)) * 2 + c

    def other(self, dp, ds):
        p, s, c = (self.s + dp + 4) % 4, (self.p + ds + 4) % 4, 1 - self.c
        return ((1 - c) * (4 * s + p) + c * (4 * p + s)) * 2 + c

    def ring(self, dx):
        return (self.me, (self.x + dx + 4) % 4)


def remote(view, send, recv, device):
    return pltpu.make_async_remote_copy(
        src_ref=view,
        dst_ref=view,
        send_sem=send,
        recv_sem=recv,
        device_id=device,
        device_id_type=MESH,
    )


class Plane:
    count = 36

    def __init__(self, place, whole, half, send, recv):
        self.at, self.whole, self.half, self.send, self.recv = place, whole, half, send, recv

    def copy(self, n):
        at = self.at
        if n < 2:
            view, to = self.whole(at.own(0, 0)), at.own(1 - 2 * n, 0)
        elif n < 4:
            view = self.half(at.own(-1 if n == 2 else 1, 0), n - 2)
            to = at.own(1 if n == 2 else -1, 0)
        elif n < 12:
            view = self.whole(at.own(OFFS[n % 4], 0))
            to = at.own(0, 1 if n < 8 else -1)
        elif n < 20:
            low = n < 16
            view = self.half(at.own(OFFS[n % 4], -1 if low else 1), 0 if low else 1)
            to = at.own(0, 1 if low else -1)
        else:
            view = self.whole(at.own(OFFS[n % 4], (0, -1, 1, 2)[(n - 20) // 4]))
            to = at.other(0, 0)
        return remote(view, self.send.at[n], self.recv.at[n], (to, at.x))

    def go(self, *ns):
        for n in ns:
            self.copy(n).start()

    def come(self, *ns):
        for n in ns:
            self.copy(n).wait_recv()

    def event(self, e):
        line, i = e // 4, e % 4
        if e == 1:
            self.come(0)
            self.go(2, 5, 9)
        elif e == 2:
            self.come(1)
            self.go(3, 6, 10)
        elif e == 3:
            self.come(2, 3)
            self.go(7, 11)
        elif line == 1:
            self.come(4 + i)
            self.go(12 + i)
        elif line == 2:
            self.come(8 + i)
            self.go(16 + i)
        else:
            self.come(12 + i, 16 + i)
        self.go(20 + e)

    def own_block(self, e):
        return self.at.own(OFFS[e % 4], (0, -1, 1, 2)[e // 4])

    def other_block(self, e):
        return self.at.other(OFFS[e % 4], (0, -1, 1, 2)[e // 4])

    def shared(self, e):
        self.come(20 + e)

    def drain(self):
        for n in range(self.count):
            self.copy(n).wait_send()


class Ring:
    def __init__(self, place, whole, half, send, recv, share):
        self.at, self.whole, self.half = place, whole, half
        self.send, self.recv, self.share = send, recv, share

    def copy(self, n):
        at = self.at
        if n < 2:
            view, to = self.whole(at.x), at.ring(1 - 2 * n)
        elif n < 4:
            view = self.half((at.x + (3 if n == 2 else 1)) % 4, n - 2)
            to = at.ring(1 if n == 2 else -1)
        else:
            view, to = self.whole((at.x + (3, 1, 2)[n - 4]) % 4), (at.other(0, 0), at.x)
        return remote(view, self.send.at[n], self.recv.at[n], to)

    def start(self):
        self.copy(0).start()
        self.copy(1).start()

    def relay(self):
        for n in (0, 1):
            self.copy(n).wait_recv()
            self.copy(n + 2).start()
            if self.share:
                self.copy(n + 4).start()

    def last(self):
        self.copy(2).wait_recv()
        self.copy(3).wait_recv()
        if self.share:
            self.copy(6).start()

    def shared(self):
        for n in (4, 5, 6):
            self.copy(n).wait_recv()

    def drain(self):
        for n in range(7 if self.share else 4):
            self.copy(n).wait_send()


RECV = (0, 1, 2, 4, 8, 3, 5, 9, 6, 10, 12, 7, 11, 13, 14, 15)
CHIPS = (
    (0, 0), (0, 1), (0, 2), (1, 0), (2, 0), (1, 1), (1, 2), (2, 1),
    (2, 2), (0, 3), (3, 0), (1, 3), (3, 1), (2, 3), (3, 2), (3, 3),
)


def pick(i, values):
    total = 0
    for k, v in enumerate(values):
        total = total + jnp.where(i == k, v, 0)
    return total


def dispatch(i, jobs, low=0):
    if len(jobs) == 1:
        jobs[0]()
        return
    mid = len(jobs) // 2

    @pl.when(i < low + mid)
    def _():
        dispatch(i, jobs[:mid], low)

    @pl.when(i >= low + mid)
    def _():
        dispatch(i, jobs[mid:], low + mid)


CHUNKS = ((0, 0), (0, 384), (1, 0), (2, 384))


def attend(blocks, q_a, q_b, peak, denom, numer, rows):
    def score(chunk):
        which, at = chunk
        q = q_a if which == 0 else q_b
        found = []
        for kv in blocks:
            key = kv[0:rows, 128 * which : 128 * (which + 1)]
            left = jnp.concatenate([key, key], 1)
            found.append(jnp.dot(left, q[:, at : at + rows], preferred_element_type=F32))
        return found

    coming = score(CHUNKS[0])
    for k, (which, at) in enumerate(CHUNKS):
        scores = coming
        if k + 1 < len(CHUNKS):
            coming = score(CHUNKS[k + 1])
        group = min(which, 1)
        cols = slice(at + 2 * rows * group, at + 2 * rows * group + rows)
        before = peak[0:1, cols]
        fresh = before
        for one in scores:
            fresh = jnp.maximum(fresh, jnp.max(one, axis=0, keepdims=True))
        decay = jnp.exp2(before - fresh)
        weights = [jnp.exp2(one - fresh) for one in scores]
        peak[0:1, cols] = fresh
        total = denom[0:1, cols] * decay
        for one in weights:
            total = total + jnp.sum(one, axis=0, keepdims=True)
        denom[0:1, cols] = total
        value = jnp.concatenate(
            [kv[rows + 128 * group : rows + 128 * (group + 1), :] for kv in blocks], 1
        )
        weights = jnp.concatenate([one.astype(BF16) for one in weights], 0)
        added = jnp.dot(value, weights, preferred_element_type=F32)
        numer[:, cols] = numer[:, cols] * decay + added


def hi_lo(q, scale):
    wide = jnp.transpose(q.astype(F32) * scale)
    high = wide.astype(BF16).astype(F32)
    return high, wide - high


def kernel(
    residual, queries_a, keys_a, values_a, queries_b, keys_b, values_b, lambdas_in, head_gain_in,
    out_a, out_b, norm_gain_in, w_gate, w_up, w_down, out_to,
    lambdas, head_gain, norm_gain, out, kv, gu, dn, ow, heads, part, came, res, q_in, v_in, q_a, q_b, peak, denom, numer,
    summed, normed, gates, hidden, square,
    kv_send, kv_recv, gu_send, gu_recv, dn_recv, ow_send, ow_recv,
    hd_send, hd_recv, rs_send, rs_recv, load, put,
):
    at = Place()
    me, x = at.me, at.x
    rows = residual.shape[0]
    depth = w_gate.shape[0]
    share = out_to.shape[1]
    inner = w_gate.shape[1]

    def local(n, src, dst):
        return pltpu.make_async_copy(src, dst, load.at[n])

    with jax.named_scope("entry"):
        loads = [
            local(0, keys_a, kv.at[me, 0:rows, 0:128]),
            local(1, keys_b, kv.at[me, 0:rows, 128:384]),
            local(2, values_a, v_in.at[0]),
            local(3, values_b, v_in.at[1]),
            local(4, queries_a, q_in.at[:, 0:128]),
            local(5, queries_b, q_in.at[:, 128:384]),
            local(6, out_a, ow.at[x, 0]),
            local(7, out_b, ow.at[x, 1]),
            local(8, w_gate, gu.at[0, me]),
            local(9, w_up, gu.at[1, me]),
            local(10, w_down, dn.at[me]),
            local(11, residual, res),
            local(12, lambdas_in, lambdas),
            local(13, head_gain_in, head_gain),
            local(14, norm_gain_in, norm_gain),
        ]
        for c in loads[:6]:
            c.start()

        barrier = pltpu.get_barrier_semaphore()
        friends = [(at.own(1, 0), x), (at.own(-1, 0), x), (at.own(0, 1), x), (at.own(0, -1), x)]
        friends += [(at.other(0, 0), x), at.ring(1), at.ring(2), at.ring(-1)]
        for f in friends:
            pl.semaphore_signal(barrier, inc=1, device_id=f, device_id_type=MESH)

        for n in (2, 3):
            loads[n].wait()
        for g in range(2):
            kv[me, rows + 128 * g : rows + 128 * (g + 1), :] = jnp.transpose(
                v_in[g].astype(F32)
            ).astype(BF16)
        for n in (0, 1):
            loads[n].wait()
        pl.semaphore_wait(barrier, len(friends))

    cut = (rows + 256) // 2
    KV = Plane(
        at, lambda b: kv.at[b], lambda b, h: kv.at[b, cut * h : cut * (h + 1)], kv_send, kv_recv
    )
    mid = depth // 2
    GU = Plane(
        at,
        lambda b: gu.at[:, b],
        lambda b, h: gu.at[:, b, mid * h : mid * (h + 1)],
        gu_send,
        gu_recv,
    )
    DN = Plane(
        at, lambda b: dn.at[b], lambda b, h: dn.at[b, mid * h : mid * (h + 1)], kv_send, dn_recv
    )
    OW = Ring(
        at,
        lambda b: ow.at[b, at.c],
        lambda b, h: ow.at[b, at.c, 64 * h : 64 * (h + 1)],
        ow_send,
        ow_recv,
        True,
    )
    HD = Ring(
        at,
        lambda b: heads.at[b],
        lambda b, h: heads.at[b, rows // 2 * h : rows // 2 * (h + 1)],
        hd_send,
        hd_recv,
        False,
    )
    with jax.named_scope("prep"):
        KV.go(0, 1, 20)
        for c in loads[6:]:
            c.start()
        for n in (6, 7):
            loads[n].wait()
        OW.start()

        for n in (4, 5):
            loads[n].wait()
        high, low = hi_lo(q_in[:, 0:128], log2e / 8.0)
        first = lax.broadcasted_iota(jnp.int32, high.shape, 0) < 64
        for j in range(2):
            keep = first if j == 0 else jnp.logical_not(first)
            cols = slice(rows * j, rows * (j + 1))
            q_a[0:128, cols] = jnp.where(keep, high, 0.0).astype(BF16)
            q_a[128:256, cols] = jnp.where(keep, low, 0.0).astype(BF16)
            high_b, low_b = hi_lo(q_in[:, 128 * (j + 1) : 128 * (j + 2)], log2e * 128.0**-0.5)
            q_b[0:128, cols] = high_b.astype(BF16)
            q_b[128:256, cols] = low_b.astype(BF16)
        peak[...] = jnp.full(peak.shape, -1e30, F32)
        denom[...] = jnp.zeros(denom.shape, F32)
        numer[...] = jnp.zeros(numer.shape, F32)
        for n in range(8, 15):
            loads[n].wait()

    def take(k):
        def job():
            if k == 1:
                KV.go(4, 8)
                KV.event(RECV[1])
            if 1 <= k < 15:
                KV.event(RECV[k + 1])
            if k == 11:
                GU.go(4, 8, 20)
            if k == 12:
                GU.go(0, 1)
            KV.shared(RECV[k])
            if k == 5:
                OW.relay()
            if k == 10:
                OW.last()

        return job

    turns = [(OFFS[e % 4] + 4) % 4 for e in RECV]
    lines = [(OFFS[e // 4] + 4) % 4 for e in RECV]

    def step(i, carry):
        with jax.named_scope("take"):
            dispatch(i, [take(k) for k in range(16)])
            dp, ds = pick(i, turns), pick(i, lines)
            blocks = [kv.at[at.own(dp, ds)], kv.at[at.other(dp, ds)]]
        with jax.named_scope("attend"):
            attend(blocks, q_a, q_b, peak, denom, numer, rows)
        return carry

    lax.fori_loop(0, 16, step, 0)

    with jax.named_scope("gu_one"):
        GU.event(1)
        GU.event(2)

    with jax.named_scope("finish"):
        ratio = numer[...] / denom[0:1, :]
        for g in range(2):
            base = 2 * rows * g
            mixed = ratio[:, base : base + rows] - lambdas[0, g] * ratio[:, base + rows : base + 2 * rows]
            scale = lax.rsqrt(jnp.mean(mixed * mixed, axis=0, keepdims=True) + eps_norm)
            done = jnp.transpose(mixed * scale) * head_gain[g : g + 1, :] * head_scale
            heads[x, :, 128 * g : 128 * (g + 1)] = done.astype(BF16)
        HD.start()

    with jax.named_scope("gu_two"):
        GU.event(4)
        GU.event(8)
    with jax.named_scope("hd_relay"):
        HD.relay()
    with jax.named_scope("gu_2b"):
        for e in (3, 5, 9):
            GU.event(e)
    with jax.named_scope("hd_last"):
        HD.last()
        OW.shared()
        wide = summed.shape[1]

    with jax.named_scope("project"):
        square[...] = jnp.zeros(square.shape, F32)

        @pl.loop(0, wide // 256)
        def _(n):
            cols = pl.ds(pl.multiple_of(n * 256, 256), 256)
            left = jnp.concatenate([heads[k] for k in range(4)], axis=1)
            right = ow[:, :, :, cols].reshape(1024, 256)
            total = res[:, cols].astype(F32) + jnp.dot(left, right, preferred_element_type=F32)
            summed[:, cols] = total
            twice = total * total
            square[...] += twice[:, 0:128] + twice[:, 128:256]

    with jax.named_scope("gu_three"):
        for e in (6, 10, 12):
            GU.event(e)

    with jax.named_scope("norm"):
        inverse = lax.rsqrt(jnp.sum(square[...], axis=1, keepdims=True) / wide + eps_norm)

        @pl.loop(0, wide // 256)
        def _(n):
            cols = pl.ds(pl.multiple_of(n * 256, 256), 256)
            normed[:, cols] = (summed[:, cols] * inverse * norm_gain[0:1, cols]).astype(BF16)

    pieces = ((0, 512), (512, 512), (1024, inner - 1024))
    with jax.named_scope("gu_four"):
        gates[...] = jnp.zeros(gates.shape, F32)
        KV.drain()
        OW.drain()
        HD.drain()

    def line(k):
        def job():
            if k == 1:
                GU.event(7)
                GU.event(11)
                DN.go(4, 8, 20, 0, 1)
            if k > 0:
                GU.event(12 + k)
            if k == 3:
                DN.event(1)
                DN.event(2)
            for other in range(4):
                GU.shared(4 * other + k)

        return job

    def gate_step(k, carry):
        with jax.named_scope("line"):
            dispatch(k, [line(n) for n in range(4)])
            s = (at.s + pick(k, (0, 3, 1, 2))) % 4
            chips = [(1 - at.c) * (4 * s + n) + at.c * (4 * n + s) for n in range(4)]
        with jax.named_scope("gate"):
            left = jnp.concatenate(
                [normed[:, pl.ds(pl.multiple_of(n * 128, 128), 128)] for n in chips], axis=1
            )
            for g in range(2):
                for lo, n in pieces:
                    right = jnp.concatenate(
                        [gu[g, pl.ds(2 * m, 2), :, lo : lo + n].reshape(128, n) for m in chips],
                        axis=0,
                    )
                    gates[g, :, lo : lo + n] += jnp.dot(left, right, preferred_element_type=F32)
        return carry

    lax.fori_loop(0, 4, gate_step, 0)

    with jax.named_scope("act"):
        for lo, n in pieces:
            gate = gates[0, :, lo : lo + n]
            hidden[:, lo : lo + n] = (
                gate / (1.0 + jnp.exp(-gate)) * gates[1, :, lo : lo + n]
            ).astype(BF16)

    with jax.named_scope("dn_one"):
        DN.event(4)
        DN.event(8)
        GU.drain()

    def give(chip):
        to, y = chip // 4, chip % 4
        slot = (to - x + 3) % 4
        return pltpu.make_async_remote_copy(
            src_ref=part.at[chip],
            dst_ref=came.at[slot, y],
            send_sem=rs_send.at[chip],
            recv_sem=rs_recv.at[4 * slot + y],
            device_id=(me, to),
            device_id_type=MESH,
        )

    down_events = ((), (), (3, 5, 9), (6, 10), (12,), (7, 11, 13), (14,), (15,))
    down_shared = ((0, 1), (2, 4), (8, 5), (6, 9), (10, 3), (12, 7), (13, 11), (14, 15))

    def arrive(k):
        def job():
            for e in down_events[k]:
                DN.event(e)
            for e in down_shared[k]:
                DN.shared(e)

        return job

    offsets = (0, 3, 1, 2)

    def down_step(k, carry):
        with jax.named_scope("arrive"):
            dispatch(k, [arrive(n) for n in range(8)])
            chips = []
            for n in range(2):
                dp = pick(k, [offsets[a] for a, _ in CHIPS[n::2]])
                ds = pick(k, [offsets[b] for _, b in CHIPS[n::2]])
                chips.append(at.own(dp, ds) // 2)
        with jax.named_scope("down"):
            right = jnp.concatenate(
                [dn[pl.ds(2 * m, 2)].reshape(128, inner) for m in chips], axis=0
            )
            sums = lax.dot_general(
                hidden[...], right, (((1,), (1,)), ((), ())), preferred_element_type=F32
            ).astype(BF16)
            for n, m in enumerate(chips):
                part[m] = sums[:, 128 * n : 128 * (n + 1)]
        with jax.named_scope("give"):
            for m in chips:

                @pl.when(m // 4 != x)
                def _(m=m):
                    give(m).start()
        return carry

    lax.fori_loop(0, 8, down_step, 0)

    with jax.named_scope("sum"):
        for y in range(4):
            total = part[4 * x + y].astype(F32)
            for slot in range(3):
                pltpu.make_async_remote_copy(
                    src_ref=part.at[y],
                    dst_ref=came.at[slot, y],
                    send_sem=rs_send.at[y],
                    recv_sem=rs_recv.at[4 * slot + y],
                    device_id=at.ring(1),
                    device_id_type=MESH,
                ).wait_recv()
                total = total + came[slot, y].astype(F32)
            cols = pl.ds(pl.multiple_of(x * share + 128 * y, 128), 128)
            out[:, 128 * y : 128 * (y + 1)] = (summed[:, cols] + 0.5 * total).astype(BF16)
        done = pltpu.make_async_copy(out, out_to, put)
        done.start()

    with jax.named_scope("drain"):
        DN.drain()
        for n in range(1, 4):
            for y in range(4):
                give(4 * ((x + n) % 4) + y).wait_send()
        done.wait()


def local(
    residual, queries_a, keys_a, values_a, queries_b, keys_b, values_b, mix_lambda, head_gain,
    out_a, out_b, norm_gain, w_gate, w_up, w_down,
):
    rows, wide = residual.shape
    depth, inner = w_gate.shape
    share = wide // 4
    anywhere = pl.BlockSpec(memory_space=pl.ANY)
    dma = pltpu.SemaphoreType.DMA
    count = Plane.count
    return pl.pallas_call(
        kernel,
        out_shape=jax.ShapeDtypeStruct((rows, share), BF16),
        in_specs=[anywhere] * 15,
        out_specs=anywhere,
        scratch_shapes=[
            pltpu.SMEM((1, 2), F32),
            pltpu.VMEM((2, 128), F32),
            pltpu.VMEM((1, wide), F32),
            pltpu.VMEM((rows, share), BF16),
            pltpu.VMEM((32, rows + 256, rows), BF16),
            pltpu.VMEM((2, 32, depth, inner), BF16),
            pltpu.VMEM((32, depth, inner), BF16),
            pltpu.VMEM((4, 2, 128, wide), BF16),
            pltpu.VMEM((4, rows, 256), BF16),
            pltpu.VMEM((16, rows, 128), BF16),
            pltpu.VMEM((3, 4, rows, 128), BF16),
            pltpu.VMEM((rows, wide), BF16),
            pltpu.VMEM((rows, 384), BF16),
            pltpu.VMEM((2, rows, 128), BF16),
            pltpu.VMEM((256, 2 * rows), BF16),
            pltpu.VMEM((256, 2 * rows), BF16),
            pltpu.VMEM((1, 4 * rows), F32),
            pltpu.VMEM((1, 4 * rows), F32),
            pltpu.VMEM((128, 4 * rows), F32),
            pltpu.VMEM((rows, wide), F32),
            pltpu.VMEM((rows, wide), BF16),
            pltpu.VMEM((2, rows, inner), F32),
            pltpu.VMEM((rows, inner), BF16),
            pltpu.VMEM((rows, 128), F32),
            dma((count,)), dma((count,)), dma((count,)), dma((count,)), dma((count,)),
            dma((7,)), dma((7,)), dma((4,)), dma((4,)), dma((16,)), dma((12,)),
            dma((15,)), dma,
        ],
        compiler_params=pltpu.CompilerParams(
            collective_id=0, has_side_effects=True, vmem_limit_bytes=67043328
        ),
        name="layer",
    )(
        residual, queries_a, keys_a, values_a, queries_b, keys_b, values_b, mix_lambda.T, head_gain,
        out_a, out_b, norm_gain.reshape(1, wide), w_gate, w_up, w_down.T,
    )


def solution(mesh):
    in_specs = (
        P("sp", None),
        P("sp", "tp"),
        P("sp", "tp"),
        P("sp", "tp"),
        P("sp", "tp"),
        P("sp", "tp"),
        P("sp", "tp"),
        P(None, "tp"),
        P(),
        P("tp", None),
        P("tp", None),
        P(),
        P("sp", "tp"),
        P("sp", "tp"),
        P("tp", "sp"),
    )
    return jax.shard_map(
        local, mesh=mesh, in_specs=in_specs, out_specs=P("sp", "tp"), check_vma=False
    )
```

time: 146 us -> 115 us (0.79); the launches traced: 144 us -> 115 us
  Pallas kernels: 139 us -> 113 us
  local copies, waits for them, and re-layouts: 4.91 us -> 1.77 us
    pallas_call x1, Pallas kernels: 139 us -> 113 us  [local(): pl.pallas_call(kernel, out_shape=jax.ShapeDtypeStruct((rows, share), BF16...]
    unnamed x3 -> x1, local copies, waits for them, and re-layouts: 4.91 us -> 1.77 us
where the time goes in v1:
time: 115 us
  Pallas kernels  113 us (98%)
  local copies, waits for them, and re-layouts  1.77 us (2%)
    pallas_call x1, Pallas kernels, local(): pl.pallas_call(kernel, out_shape=jax.ShapeDtypeStruct((rows, share), BF16...  113 us

profile of v1, /device:TPU:5, one launch (start us, length us, event | category | flops | bytes accessed | tf_op | source)
XLA Modules:
  0.0 114.6 jit_solution(10039261772706955057)
XLA Ops:
  0.0 112.8 %layer.1 = bf16[384,512]{1,0:T(8,128)(2,1)} custom-call(bf16[384,2048]{1,0:T(8,128)(2,1)} %residual.1, bf16[384,128]{1,0:T(8,128)(2,1)} %queries_a.1, bf16[384,128]{1,0:T(8,128)(2,1)} %keys_a.1, bf16[384,128]{1,0:T(8,128)(2,1)} %values_a.1, bf16[384,256]{1,0:T(8,128)(2,1)} %queries_b.1, bf16[384,256]{1,0:T(8,128)(2,1)} %keys_b.1, bf16[384,128]{1,0:T(8,128)(2,1)} %values_b.1, ...), custom_call_target="tpu_custom_call" | custom-call | tf_op jit(solution)/shard_map/layer/pallas_call | solution.py:579
  112.8 1.8 %copy.17 = bf16[384,512]{1,0:T(8,128)(2,1)} copy(bf16[384,512]{1,0:T(8,128)(2,1)} %layer.1) | data formatting | bytes 786432

commit v2 on v1

--- a/solution.py
+++ b/solution.py
@@ -165,6 +165,9 @@
     (0, 0), (0, 1), (0, 2), (1, 0), (2, 0), (1, 1), (1, 2), (2, 1),
     (2, 2), (0, 3), (3, 0), (1, 3), (3, 1), (2, 3), (3, 2), (3, 3),
 )
+
+
+LAG = 3
 
 
 def pick(i, values):
@@ -237,17 +240,17 @@
 
 def kernel(
     residual, queries_a, keys_a, values_a, queries_b, keys_b, values_b, lambdas_in, head_gain_in,
-    out_a, out_b, norm_gain_in, w_gate, w_up, w_down, out_to,
-    lambdas, head_gain, norm_gain, out, kv, gu, dn, ow, heads, part, came, res, q_in, v_in, q_a, q_b, peak, denom, numer,
+    out_a, out_b, norm_gain_in, w_gate, w_up, w_down, out,
+    lambdas, head_gain, norm_gain, kv, gu, dn, ow, heads, part, came, passing, res, q_in, v_in, q_a, q_b, peak, denom, numer,
     summed, normed, gates, hidden, square,
     kv_send, kv_recv, gu_send, gu_recv, dn_recv, ow_send, ow_recv,
-    hd_send, hd_recv, rs_send, rs_recv, load, put,
+    hd_send, hd_recv, rs_send, rs_recv, ps_recv, load,
 ):
     at = Place()
     me, x = at.me, at.x
     rows = residual.shape[0]
     depth = w_gate.shape[0]
-    share = out_to.shape[1]
+    share = out.shape[1]
     inner = w_gate.shape[1]
 
     def local(n, src, dst):
@@ -322,7 +325,7 @@
         False,
     )
     with jax.named_scope("prep"):
-        KV.go(0, 1, 20)
+        KV.go(0, 1, 4, 8, 20)
         for c in loads[6:]:
             c.start()
         for n in (6, 7):
@@ -350,7 +353,6 @@
     def take(k):
         def job():
             if k == 1:
-                KV.go(4, 8)
                 KV.event(RECV[1])
             if 1 <= k < 15:
                 KV.event(RECV[k + 1])
@@ -487,17 +489,53 @@
         DN.event(8)
         GU.drain()
 
-    def give(chip):
-        to, y = chip // 4, chip % 4
-        slot = (to - x + 3) % 4
+    half = rows // 2
+
+    def give(chip, h, to, target, arrived, n):
         return pltpu.make_async_remote_copy(
-            src_ref=part.at[chip],
-            dst_ref=came.at[slot, y],
-            send_sem=rs_send.at[chip],
-            recv_sem=rs_recv.at[4 * slot + y],
+            src_ref=part.at[chip, half * h : half * (h + 1)],
+            dst_ref=target,
+            send_sem=rs_send.at[2 * chip + n],
+            recv_sem=arrived,
             device_id=(me, to),
             device_id_type=MESH,
         )
+
+    def side(chip, n, h):
+        y = chip % 4
+        target = came.at[n, y, half * h : half * (h + 1)]
+        return give(chip, h, chip // 4, target, rs_recv.at[8 * n + 2 * y + h], h)
+
+    def through(chip, n):
+        y = chip % 4
+        return give(chip, n, (x + 1 + 2 * n) % 4, passing.at[n, y], ps_recv.at[4 * n + y], n)
+
+    def first_give(chip):
+        away = (chip // 4 - x + 4) % 4
+
+        @pl.when(away == 2)
+        def _():
+            through(chip, 0).start()
+            through(chip, 1).start()
+
+        for n in range(2):
+
+            @pl.when(away == 1 + 2 * n)
+            def _(n=n):
+                side(chip, n, 1 - n).start()
+
+    def second_give(chip):
+        y = chip % 4
+        away = (chip // 4 - x + 4) % 4
+        for n in range(2):
+
+            @pl.when(away == 1 + 2 * n)
+            def _(n=n):
+                through(chip, n).wait_recv()
+                mine = part[chip, half * n : half * (n + 1)].astype(F32)
+                mine = mine + passing[n, y].astype(F32)
+                part[chip, half * n : half * (n + 1)] = mine.astype(BF16)
+                side(chip, n, n).start()
 
     down_events = ((), (), (3, 5, 9), (6, 10), (12,), (7, 11, 13), (14,), (15,))
     down_shared = ((0, 1), (2, 4), (8, 5), (6, 9), (10, 3), (12, 7), (13, 11), (14, 15))
@@ -513,14 +551,18 @@
 
     offsets = (0, 3, 1, 2)
 
+    def chips_of(k):
+        found = []
+        for n in range(2):
+            dp = pick(k, [offsets[a] for a, _ in CHIPS[n::2]])
+            ds = pick(k, [offsets[b] for _, b in CHIPS[n::2]])
+            found.append(at.own(dp, ds) // 2)
+        return found
+
     def down_step(k, carry):
         with jax.named_scope("arrive"):
             dispatch(k, [arrive(n) for n in range(8)])
-            chips = []
-            for n in range(2):
-                dp = pick(k, [offsets[a] for a, _ in CHIPS[n::2]])
-                ds = pick(k, [offsets[b] for _, b in CHIPS[n::2]])
-                chips.append(at.own(dp, ds) // 2)
+            chips = chips_of(k)
         with jax.named_scope("down"):
             right = jnp.concatenate(
                 [dn[pl.ds(2 * m, 2)].reshape(128, inner) for m in chips], axis=0
@@ -532,38 +574,54 @@
                 part[m] = sums[:, 128 * n : 128 * (n + 1)]
         with jax.named_scope("give"):
             for m in chips:
-
-                @pl.when(m // 4 != x)
+                first_give(m)
+
+        with jax.named_scope("second"):
+
+            @pl.when(k >= LAG)
+            def _():
+                for m in chips_of(k - LAG):
+                    second_give(m)
+
+        return carry
+
+    lax.fori_loop(0, 8, down_step, 0)
+
+    with jax.named_scope("late"):
+
+        @pl.loop(8 - LAG, 8)
+        def _(k):
+            for m in chips_of(k):
+                second_give(m)
+
+    with jax.named_scope("sum"):
+
+        def sum_step(k, carry):
+            for m in chips_of(k):
+
+                @pl.when(m // 4 == x)
                 def _(m=m):
-                    give(m).start()
-        return carry
-
-    lax.fori_loop(0, 8, down_step, 0)
-
-    with jax.named_scope("sum"):
-        for y in range(4):
-            total = part[4 * x + y].astype(F32)
-            for slot in range(3):
-                pltpu.make_async_remote_copy(
-                    src_ref=part.at[y],
-                    dst_ref=came.at[slot, y],
-                    send_sem=rs_send.at[y],
-                    recv_sem=rs_recv.at[4 * slot + y],
-                    device_id=at.ring(1),
-                    device_id_type=MESH,
-                ).wait_recv()
-                total = total + came[slot, y].astype(F32)
-            cols = pl.ds(pl.multiple_of(x * share + 128 * y, 128), 128)
-            out[:, 128 * y : 128 * (y + 1)] = (summed[:, cols] + 0.5 * total).astype(BF16)
-        done = pltpu.make_async_copy(out, out_to, put)
-        done.start()
+                    y = m % 4
+                    cols = pl.ds(pl.multiple_of(x * share + 128 * y, 128), 128)
+                    into = pl.ds(pl.multiple_of(128 * y, 128), 128)
+                    for n in range(2):
+                        for h in range(2):
+                            side(m, n, h).wait_recv()
+                    total = (
+                        part[m].astype(F32) + came[0, y].astype(F32) + came[1, y].astype(F32)
+                    )
+                    out[:, into] = (summed[:, cols] + 0.5 * total).astype(BF16)
+
+            return carry
+
+        lax.fori_loop(0, 8, sum_step, 0)
 
     with jax.named_scope("drain"):
         DN.drain()
         for n in range(1, 4):
             for y in range(4):
-                give(4 * ((x + n) % 4) + y).wait_send()
-        done.wait()
+                for h in range(2):
+                    side(4 * ((x + n) % 4) + y, 0, h).wait_send()
 
 
 def local(
@@ -578,21 +636,21 @@
     count = Plane.count
     return pl.pallas_call(
         kernel,
-        out_shape=jax.ShapeDtypeStruct((rows, share), BF16),
+        out_shape=pltpu.VMEM((rows, share), BF16),
         in_specs=[anywhere] * 15,
-        out_specs=anywhere,
+        out_specs=pl.BlockSpec(memory_space=pltpu.VMEM),
         scratch_shapes=[
             pltpu.SMEM((1, 2), F32),
             pltpu.VMEM((2, 128), F32),
             pltpu.VMEM((1, wide), F32),
-            pltpu.VMEM((rows, share), BF16),
             pltpu.VMEM((32, rows + 256, rows), BF16),
             pltpu.VMEM((2, 32, depth, inner), BF16),
             pltpu.VMEM((32, depth, inner), BF16),
             pltpu.VMEM((4, 2, 128, wide), BF16),
             pltpu.VMEM((4, rows, 256), BF16),
             pltpu.VMEM((16, rows, 128), BF16),
-            pltpu.VMEM((3, 4, rows, 128), BF16),
+            pltpu.VMEM((2, 4, rows, 128), BF16),
+            pltpu.VMEM((2, 4, rows // 2, 128), BF16),
             pltpu.VMEM((rows, wide), BF16),
             pltpu.VMEM((rows, 384), BF16),
             pltpu.VMEM((2, rows, 128), BF16),
@@ -607,11 +665,11 @@
             pltpu.VMEM((rows, inner), BF16),
             pltpu.VMEM((rows, 128), F32),
             dma((count,)), dma((count,)), dma((count,)), dma((count,)), dma((count,)),
-            dma((7,)), dma((7,)), dma((4,)), dma((4,)), dma((16,)), dma((12,)),
-            dma((15,)), dma,
+            dma((7,)), dma((7,)), dma((4,)), dma((4,)), dma((32,)), dma((16,)), dma((8,)),
+            dma((15,)),
         ],
         compiler_params=pltpu.CompilerParams(
-            collective_id=0, has_side_effects=True, vmem_limit_bytes=67043328
+            collective_id=0, has_side_effects=True, vmem_limit_bytes=66 * 1000 * 1000
         ),
         name="layer",
     )(

time: 115 us -> 109 us (0.948)
  Pallas kernels: 113 us -> 108 us
    pallas_call x1, Pallas kernels: 113 us -> 108 us  [local(): pl.pallas_call(kernel, out_shape=pltpu.VMEM((rows, share), BF16), in_spec...]
where the time goes in v2:
time: 109 us
  Pallas kernels  108 us (99%)
    pallas_call x1, Pallas kernels, local(): pl.pallas_call(kernel, out_shape=pltpu.VMEM((rows, share), BF16), in_spec...  108 us

profile of v2, /device:TPU:5, one launch (start us, length us, event | category | flops | bytes accessed | tf_op | source)
XLA Modules:
  0.0 108.9 jit_solution(9448551759774604000)
XLA Ops:
  0.0 108.1 %layer.1 = bf16[384,512]{1,0:T(8,128)(2,1)S(1)} custom-call(bf16[384,2048]{1,0:T(8,128)(2,1)} %residual.1, bf16[384,128]{1,0:T(8,128)(2,1)} %queries_a.1, bf16[384,128]{1,0:T(8,128)(2,1)} %keys_a.1, bf16[384,128]{1,0:T(8,128)(2,1)} %values_a.1, bf16[384,256]{1,0:T(8,128)(2,1)} %queries_b.1, bf16[384,256]{1,0:T(8,128)(2,1)} %keys_b.1, ...), custom_call_target="tpu_custom_call" | custom-call | tf_op jit(solution)/shard_map/layer/pallas_call | solution.py:637
  108.1 0.7 copy.17

commit v3 on v2

--- a/solution.py
+++ b/solution.py
@@ -73,7 +73,7 @@
         else:
             view = self.whole(at.own(OFFS[n % 4], (0, -1, 1, 2)[(n - 20) // 4]))
             to = at.other(0, 0)
-        return remote(view, self.send.at[n], self.recv.at[n], (to, at.x))
+        return remote(view, self.send, self.recv.at[n], (to, at.x))
 
     def go(self, *ns):
         for n in ns:
@@ -113,9 +113,8 @@
     def shared(self, e):
         self.come(20 + e)
 
-    def drain(self):
-        for n in range(self.count):
-            self.copy(n).wait_send()
+    def drain(self, sent):
+        remote(sent, self.send, self.recv.at[0], (self.at.other(0, 0), self.at.x)).wait_send()
 
 
 class Ring:
@@ -132,7 +131,7 @@
             to = at.ring(1 if n == 2 else -1)
         else:
             view, to = self.whole((at.x + (3, 1, 2)[n - 4]) % 4), (at.other(0, 0), at.x)
-        return remote(view, self.send.at[n], self.recv.at[n], to)
+        return remote(view, self.send, self.recv.at[n], to)
 
     def start(self):
         self.copy(0).start()
@@ -155,9 +154,8 @@
         for n in (4, 5, 6):
             self.copy(n).wait_recv()
 
-    def drain(self):
-        for n in range(7 if self.share else 4):
-            self.copy(n).wait_send()
+    def drain(self, sent):
+        remote(sent, self.send, self.recv.at[0], self.at.ring(1)).wait_send()
 
 
 RECV = (0, 1, 2, 4, 8, 3, 5, 9, 6, 10, 12, 7, 11, 13, 14, 15)
@@ -243,7 +241,7 @@
     out_a, out_b, norm_gain_in, w_gate, w_up, w_down, out,
     lambdas, head_gain, norm_gain, kv, gu, dn, ow, heads, part, came, passing, res, q_in, v_in, q_a, q_b, peak, denom, numer,
     summed, normed, gates, hidden, square,
-    kv_send, kv_recv, gu_send, gu_recv, dn_recv, ow_send, ow_recv,
+    kv_send, kv_recv, gu_send, gu_recv, dn_send, dn_recv, ow_send, ow_recv,
     hd_send, hd_recv, rs_send, rs_recv, ps_recv, load,
 ):
     at = Place()
@@ -306,7 +304,7 @@
         gu_recv,
     )
     DN = Plane(
-        at, lambda b: dn.at[b], lambda b, h: dn.at[b, mid * h : mid * (h + 1)], kv_send, dn_recv
+        at, lambda b: dn.at[b], lambda b, h: dn.at[b, mid * h : mid * (h + 1)], dn_send, dn_recv
     )
     OW = Ring(
         at,
@@ -437,9 +435,9 @@
     pieces = ((0, 512), (512, 512), (1024, inner - 1024))
     with jax.named_scope("gu_four"):
         gates[...] = jnp.zeros(gates.shape, F32)
-        KV.drain()
-        OW.drain()
-        HD.drain()
+        KV.drain(kv.at[0:31])
+        OW.drain(ow.at[0:3])
+        HD.drain(heads.at[0:3])
 
     def line(k):
         def job():
@@ -487,15 +485,15 @@
     with jax.named_scope("dn_one"):
         DN.event(4)
         DN.event(8)
-        GU.drain()
+        GU.drain(gu.at[:, 0:31])
 
     half = rows // 2
 
-    def give(chip, h, to, target, arrived, n):
+    def give(chip, h, to, target, arrived):
         return pltpu.make_async_remote_copy(
             src_ref=part.at[chip, half * h : half * (h + 1)],
             dst_ref=target,
-            send_sem=rs_send.at[2 * chip + n],
+            send_sem=rs_send,
             recv_sem=arrived,
             device_id=(me, to),
             device_id_type=MESH,
@@ -504,11 +502,11 @@
     def side(chip, n, h):
         y = chip % 4
         target = came.at[n, y, half * h : half * (h + 1)]
-        return give(chip, h, chip // 4, target, rs_recv.at[8 * n + 2 * y + h], h)
+        return give(chip, h, chip // 4, target, rs_recv.at[8 * n + 2 * y + h])
 
     def through(chip, n):
         y = chip % 4
-        return give(chip, n, (x + 1 + 2 * n) % 4, passing.at[n, y], ps_recv.at[4 * n + y], n)
+        return give(chip, n, (x + 1 + 2 * n) % 4, passing.at[n, y], ps_recv.at[4 * n + y])
 
     def first_give(chip):
         away = (chip // 4 - x + 4) % 4
@@ -617,11 +615,8 @@
         lax.fori_loop(0, 8, sum_step, 0)
 
     with jax.named_scope("drain"):
-        DN.drain()
-        for n in range(1, 4):
-            for y in range(4):
-                for h in range(2):
-                    side(4 * ((x + n) % 4) + y, 0, h).wait_send()
+        DN.drain(dn.at[0:31])
+        remote(part.at[0:12], rs_send, rs_recv.at[0], at.ring(1)).wait_send()
 
 
 def local(
@@ -664,8 +659,8 @@
             pltpu.VMEM((2, rows, inner), F32),
             pltpu.VMEM((rows, inner), BF16),
             pltpu.VMEM((rows, 128), F32),
-            dma((count,)), dma((count,)), dma((count,)), dma((count,)), dma((count,)),
-            dma((7,)), dma((7,)), dma((4,)), dma((4,)), dma((32,)), dma((16,)), dma((8,)),
+            dma, dma((count,)), dma, dma((count,)), dma, dma((count,)),
+            dma, dma((7,)), dma, dma((4,)), dma, dma((16,)), dma((8,)),
             dma((15,)),
         ],
         compiler_params=pltpu.CompilerParams(

time: 109 us -> 108 us (level)
    pallas_call x1, Pallas kernels: 108 us -> 107 us  [local(): pl.pallas_call(kernel, out_shape=pltpu.VMEM((rows, share), BF16), in_spec...]
where the time goes in v3:
time: 108 us
  Pallas kernels  107 us (99%)
    pallas_call x1, Pallas kernels, local(): pl.pallas_call(kernel, out_shape=pltpu.VMEM((rows, share), BF16), in_spec...  107 us

profile of v3, /device:TPU:5, one launch (start us, length us, event | category | flops | bytes accessed | tf_op | source)
XLA Modules:
  0.0 107.8 jit_solution(9010292768393375254)
XLA Ops:
  0.0 107.0 %layer.1 = bf16[384,512]{1,0:T(8,128)(2,1)S(1)} custom-call(bf16[384,2048]{1,0:T(8,128)(2,1)} %residual.1, bf16[384,128]{1,0:T(8,128)(2,1)} %queries_a.1, bf16[384,128]{1,0:T(8,128)(2,1)} %keys_a.1, bf16[384,128]{1,0:T(8,128)(2,1)} %values_a.1, bf16[384,256]{1,0:T(8,128)(2,1)} %queries_b.1, bf16[384,256]{1,0:T(8,128)(2,1)} %keys_b.1, ...), custom_call_target="tpu_custom_call" | custom-call | tf_op jit(solution)/shard_map/layer/pallas_call | solution.py:632
  107.0 0.7 copy.17

commit v4 on v3

--- a/solution.py
+++ b/solution.py
@@ -354,10 +354,8 @@
                 KV.event(RECV[1])
             if 1 <= k < 15:
                 KV.event(RECV[k + 1])
-            if k == 11:
-                GU.go(4, 8, 20)
             if k == 12:
-                GU.go(0, 1)
+                GU.go(0, 1, 4, 8, 20)
             KV.shared(RECV[k])
             if k == 5:
                 OW.relay()
@@ -444,7 +442,7 @@
             if k == 1:
                 GU.event(7)
                 GU.event(11)
-                DN.go(4, 8, 20, 0, 1)
+                DN.go(0, 1, 4, 8, 20)
             if k > 0:
                 GU.event(12 + k)
             if k == 3:

time: 108 us -> 108 us (level)
  no operation moved by 1% of the time
where the time goes in v4:
time: 108 us; the launch traced here: 107 us
  Pallas kernels  107 us (99%)
    pallas_call x1, Pallas kernels, local(): pl.pallas_call(kernel, out_shape=pltpu.VMEM((rows, share), BF16), in_spec...  107 us

profile of v4, /device:TPU:5, one launch (start us, length us, event | category | flops | bytes accessed | tf_op | source)
XLA Modules:
  0.0 107.5 jit_solution(5089655227560979230)
XLA Ops:
  0.0 106.7 %layer.1 = bf16[384,512]{1,0:T(8,128)(2,1)S(1)} custom-call(bf16[384,2048]{1,0:T(8,128)(2,1)} %residual.1, bf16[384,128]{1,0:T(8,128)(2,1)} %queries_a.1, bf16[384,128]{1,0:T(8,128)(2,1)} %keys_a.1, bf16[384,128]{1,0:T(8,128)(2,1)} %values_a.1, bf16[384,256]{1,0:T(8,128)(2,1)} %queries_b.1, bf16[384,256]{1,0:T(8,128)(2,1)} %keys_b.1, ...), custom_call_target="tpu_custom_call" | custom-call | tf_op jit(solution)/shard_map/layer/pallas_call | solution.py:630
  106.7 0.7 copy.17
